TPU v7x, 32 devices: a whole 2x2x4 slice. The times are simulated.
32 devices in a mesh: sp: 8 (over z, y), tp: 4 (over x, core).
Axes of the slice: x: 2, y: 2, z: 4, core: 2. Of those that a mesh axis runs over, the one named last changes fastest.
Arguments:
- queries: bfloat16 [4096, 1024], P('sp', 'tp'), may hold values from -200 to 200
- keys: bfloat16 [4096, 1024], P('sp', 'tp'), may hold values from -6 to 6
- values: bfloat16 [4096, 1024], P('sp', 'tp'), may hold values from -24 to 24
- cum_gate: float32 [4096, 8], P('sp', 'tp'), may hold values from -414 to 0, as said below
- residual: bfloat16 [4096, 2048], P(('sp', 'tp')), may hold values from -1.5 to 1.5
- w_out: bfloat16 [1024, 2048], replicated, may hold values from -0.1875 to 0.1875
- gain: float32 [2048], replicated, may hold values from 0.1 to 1.9
- w_up: bfloat16 [2048, 8192], P('sp', 'tp'), may hold values from -0.125 to 0.125
- w_down: bfloat16 [8192, 2048], P('tp', 'sp'), may hold values from -0.0625 to 0.0625
Outputs:
- output: bfloat16 [4096, 2048], P(('sp', 'tp'))
Inputs may be any that keep to these rules, and one draw needn't show every extreme that they name: Within each head, cum_gate never rises from one position to the next.
All inputs are finite; a program needn't handle non-finite values.
Results may differ from a plain program's by a relative error of at most 0.022.
Values may be sent and summed in bfloat16 or wider, within the bound.
A program may use at most 128 MiB of HBM per device.

v0:
```python
import math
import jax
import jax.numpy as jnp
from jax import lax
from jax.sharding import PartitionSpec as P


def per_device(queries, keys, values, cum_gate, residual, w_out, gain, w_up, w_down):
    tok_rows, width = queries.shape
    heads_here = cum_gate.shape[1]
    head_size = width // heads_here
    score_scale = head_size ** (-0.5)
    row_offset = lax.axis_index("sp") * tok_rows
    query_heads = queries.reshape(tok_rows, heads_here, head_size)
    query_pos = row_offset + jnp.arange(tok_rows, dtype=jnp.int32)
    all_gates = lax.all_gather(cum_gate, "sp", axis=0, tiled=True)
    initial = (
        jnp.full((tok_rows, heads_here), -1e30, jnp.float32),
        jnp.zeros((tok_rows, heads_here), jnp.float32),
        jnp.zeros((tok_rows, heads_here, head_size), jnp.float32),
    )
    carried = initial
    key_rows = lax.all_gather(keys, "sp", axis=0, tiled=True)
    value_rows = lax.all_gather(values, "sp", axis=0, tiled=True)
    row_count = key_rows.shape[0]
    span_rows = math.gcd(row_count, 2048)
    block_count = row_count // span_rows
    key_blocks = key_rows.reshape(block_count, span_rows, heads_here, head_size)
    value_blocks = value_rows.reshape(block_count, span_rows, heads_here, head_size)
    first_pos = jnp.arange(block_count, dtype=jnp.int32) * span_rows

    def absorb_block(running, packed):
        running_max, running_sum, accumulated = running
        key_blk, value_blk, block_start = packed
        gate_blk = lax.dynamic_slice_in_dim(all_gates, block_start, span_rows, 0)
        scores = jnp.einsum(
            "qhd,khd->qhk", query_heads, key_blk, preferred_element_type=jnp.float32
        )
        scores = scores * score_scale + cum_gate[:, :, None] - gate_blk.T[None, :, :]
        key_pos = block_start + jnp.arange(span_rows, dtype=jnp.int32)
        scores = jnp.where(key_pos[None, None, :] <= query_pos[:, None, None], scores, -1e30)
        new_max = jnp.maximum(running_max, jnp.max(scores, axis=-1))
        rescale = jnp.exp(running_max - new_max)
        weights = jnp.exp(scores - new_max[:, :, None])
        running_sum = running_sum * rescale + jnp.sum(weights, axis=-1)
        product = jnp.einsum(
            "qhk,khd->qhd",
            weights.astype(jnp.bfloat16),
            value_blk,
            preferred_element_type=jnp.float32,
        )
        accumulated = accumulated * rescale[:, :, None] + product
        return ((new_max, running_sum, accumulated), None)

    carried, _ = lax.scan(absorb_block, carried, (key_blocks, value_blocks, first_pos))
    running_max, running_sum, accumulated = carried
    attended = (accumulated / running_sum[:, :, None]).reshape(tok_rows, width).astype(jnp.bfloat16)
    mine = lax.all_to_all(attended, "tp", split_axis=0, concat_axis=1, tiled=True)
    projected = jnp.dot(mine, w_out, preferred_element_type=jnp.float32)
    residual_sum = residual.astype(jnp.float32) + projected
    mean_square = jnp.mean(residual_sum * residual_sum, axis=-1, keepdims=True)
    normed = (residual_sum * lax.rsqrt(mean_square + 1e-06) * gain).astype(jnp.bfloat16)
    normed_all = lax.all_gather(normed, "tp", axis=0, tiled=True)
    up_proj = jnp.dot(
        normed_all,
        lax.all_gather(w_up, "sp", axis=0, tiled=True),
        preferred_element_type=jnp.float32,
    )
    hidden = jnp.square(jax.nn.relu(up_proj)).astype(jnp.bfloat16)
    down_whole = lax.all_gather(w_down, "sp", axis=1, tiled=True)
    rounded = jnp.dot(hidden, down_whole, preferred_element_type=jnp.float32).astype(jnp.bfloat16)
    branch_out = lax.psum_scatter(
        lax.optimization_barrier(rounded).astype(jnp.float32).astype(jnp.bfloat16),
        "tp",
        scatter_dimension=0,
        tiled=True,
    ).astype(jnp.float32)
    return (residual_sum + branch_out).astype(jnp.bfloat16)


def solution(mesh):
    return jax.shard_map(
        per_device,
        mesh=mesh,
        in_specs=(
            P("sp", "tp"),
            P("sp", "tp"),
            P("sp", "tp"),
            P("sp", "tp"),
            P(("sp", "tp"), None),
            P(),
            P(),
            P("sp", "tp"),
            P("tp", "sp"),
        ),
        out_specs=P(("sp", "tp"), None),
        check_vma=False,
    )
```

profile of v0, /device:TPU:0, one launch (start us, length us, event | category | flops | bytes accessed | tf_op | source)
XLA Modules:
  0.0 501.9 jit_solution(15590965651173478988)
XLA Ops:
  6.5 0.0 copy-start
  6.5 0.0 all-gather.6.cloned.1.call-start
  6.5 0.7 all-gather.6.cloned.1.call-update
  7.3 0.0 all-gather.8.cloned.1.call-start
  7.3 0.7 all-gather.8.cloned.1.call-update
  8.0 0.0 all-gather.10.cloned.1.call-start
  8.1 1.1 copy.17
  9.2 0.2 copy.19
  9.4 32.7 %all_gather.19 = f32[4096,2]{0,1:T(2,128)S(1)} all-gather(f32[512,2]{0,1:T(2,128)} %param.14), channel_id=1, replica_groups=mesh['sp'=8,'tp'=4] {'sp'}, dimensions={0}, use_global_device_ids=true | all-gather | bytes 36864 | tf_op jit(solution)/shard_map/all_gather | solution.py:16
  42.0 19.4 %all-gather.6.cloned.1.call-done = bf16[4096,256]{1,0:T(8,128)(2,1)} async-done(((bf16[512,256]{1,0:T(8,128)(2,1)}), bf16[4096,256]{1,0:T(8,128)(2,1)}) %all-gather.6.cloned.1.call-update) | async-done | bytes 2097168 | tf_op jit(solution)/shard_map/all_gather | solution.py:23
  61.4 4.0 reshape.62
  65.4 45.8 %all-gather.8.cloned.1.call-done = bf16[4096,256]{1,0:T(8,128)(2,1)} async-done(((bf16[512,256]{1,0:T(8,128)(2,1)}), bf16[4096,256]{1,0:T(8,128)(2,1)}) %all-gather.8.cloned.1.call-update) | async-done | bytes 2097168 | tf_op jit(solution)/shard_map/all_gather | solution.py:24
  111.2 4.0 reshape.64
  115.2 0.0 copy-done
  115.2 45.9 %while.15 = (s32[]{:T(128)}, f32[512,2]{0,1:T(2,128)S(1)}, f32[512,2]{0,1:T(2,128)S(1)}, f32[512,2,128]{0,2,1:T(8,128)}, s32[2]{0:T(128)S(1)}, /*index=5*/bf16[2...) while((s32[]{:T(128)}, f32[512,2]{0,1:T(2,128)S(1)}, ...), condition=%wide.region_3.4_spmd.clone, body=%wide.region_0.3_spmd.clone.sunk | while | flops 1110842880 | bytes 39239884 | solution.py:55
  115.2 0.6 dynamic_slice.26
  117.4 0.1 dynamic-slice_bitcast_fusion.2
  117.5 0.6 iota_add_fusion.5
  118.1 0.8 broadcast_compare_fusion.2
  118.9 2.7 constant_dynamic-slice_fusion.3
  121.6 4.6 fusion.40
  126.2 4.8 fusion.42
  131.0 0.8 copy.34
  131.8 6.2 %fusion.44 = f32[512,2,128]{0,2,1:T(8,128)} fusion(f32[2,2048,512]{2,1,0:T(8,128)} %get-tuple-element.231, f32[512,2]{0,1:T(2,128)S(1)} %fusion.41, f32[2,2048]{1,0:T(2,128)S(1)} %dynamic-slice_bitcast_fusion.2, f32[512,2]{0,1:T(2,128)S(1)} %get-tuple-element.270, pred[512,2048]{0,1:T(8,128)(4,1)S(1)} %broadcast_compare_fusion.2, ...), kind=kOutput, calls=%fused_computation.12.clone.1 | convolution fusion | flops 549847040 | bytes 11563009 | tf_op jit(solution)/shard_map/while/body/eval_jaxpr/qhk,khd->qhd/dot_general | solution.py:46
  138.1 0.6 dynamic_slice.26
  140.3 0.1 dynamic-slice_bitcast_fusion.2
  140.4 0.6 iota_add_fusion.5
  141.0 0.8 broadcast_compare_fusion.2
  141.8 2.7 constant_dynamic-slice_fusion.3
  144.5 4.6 fusion.40
  149.1 4.8 fusion.42
  153.9 0.8 copy.34
  154.7 6.4 %fusion.44 = f32[512,2,128]{0,2,1:T(8,128)} fusion(f32[2,2048,512]{2,1,0:T(8,128)} %get-tuple-element.231, f32[512,2]{0,1:T(2,128)S(1)} %fusion.41, f32[2,2048]{1,0:T(2,128)S(1)} %dynamic-slice_bitcast_fusion.2, f32[512,2]{0,1:T(2,128)S(1)} %get-tuple-element.270, pred[512,2048]{0,1:T(8,128)(4,1)S(1)} %broadcast_compare_fusion.2, ...), kind=kOutput, calls=%fused_computation.12.clone.1 | convolution fusion | flops 549847040 | bytes 11563009 | tf_op jit(solution)/shard_map/while/body/eval_jaxpr/qhk,khd->qhd/dot_general | solution.py:46
  161.1 0.0 copy-start.1
  161.1 1.1 divide_convert_fusion
  162.2 0.1 reshape.65
  162.2 0.2 copy.24
  162.4 8.5 %all_to_all.16 = bf16[4,128,256]{2,1,0:T(8,128)(2,1)S(1)} all-to-all(bf16[4,128,256]{2,1,0:T(8,128)(2,1)S(1)} %copy.24), channel_id=1, replica_groups=mesh['sp'=8,'tp'=4] {'tp'}, dimensions={0} | all-to-all | bytes 524288 | tf_op jit(solution)/shard_map/all_to_all | solution.py:58
  171.0 0.2 copy.22
  171.1 3.1 multiply_reduce_fusion
  174.3 0.0 copy-done.1
  174.3 0.9 multiply_convert_fusion.1
  175.2 0.0 all-gather.10.cloned.1.call-update
  175.3 0.0 all-gather.12.cloned.1.call-start
  175.3 0.5 all-gather.12.cloned.1.call-update
  175.8 0.0 all-gather.14.cloned.1.call-start
  175.9 0.5 all-gather.14.cloned.1.call-update
  176.4 0.2 reduce-scatter.2.cloned.1.call-start
  176.7 19.0 %all-gather.10.cloned.1.call-done = bf16[512,2048]{1,0:T(8,128)(2,1)} async-done(((bf16[128,2048]{1,0:T(8,128)(2,1)}), bf16[512,2048]{1,0:T(8,128)(2,1)}) %all-gather.10.cloned.1.call-update) | async-done | bytes 2097168 | tf_op jit(solution)/shard_map/all_gather | solution.py:63
  195.6 126.5 %all-gather.12.cloned.1.call-done = bf16[2048,2048]{1,0:T(8,128)(2,1)} async-done(((bf16[256,2048]{1,0:T(8,128)(2,1)}), bf16[2048,2048]{1,0:T(8,128)(2,1)}) %all-gather.12.cloned.1.call-update) | async-done | bytes 8388624 | tf_op jit(solution)/shard_map/all_gather | solution.py:66
  322.1 125.0 %all-gather.14.cloned.1.call-done = bf16[2048,2048]{1,0:T(8,128)(2,1)} async-done(((bf16[2048,256]{1,0:T(8,128)(2,1)}), bf16[2048,2048]{1,0:T(8,128)(2,1)}) %all-gather.14.cloned.1.call-update) | async-done | bytes 8388624 | tf_op jit(solution)/shard_map/all_gather | solution.py:70
  447.1 16.5 %convolution_convert_fusion = bf16[512,2048]{1,0:T(8,128)(2,1)} fusion(bf16[2048,2048]{1,0:T(8,128)(2,1)} %all-gather.14.cloned.1.call-done, bf16[512,2048]{1,0:T(8,128)(2,1)} %all-gather.10.cloned.1.call-done, bf16[2048,2048]{1,0:T(8,128)(2,1)} %all-gather.12.cloned.1.call-done), kind=kOutput, calls=%fused_computation.30 | convolution fusion | flops 8594128896 | bytes 20971520 | tf_op jit(solution)/shard_map/dot_general | solution.py:71
  463.7 0.0 reduce-scatter.2.cloned.1.call-update
  463.7 29.5 %reduce-scatter.2.cloned.1.call-done = bf16[128,2048]{1,0:T(8,128)(2,1)} async-done(((bf16[512,2048]{1,0:T(8,128)(2,1)}), bf16[128,2048]{1,0:T(8,128)(2,1)}) %reduce-scatter.2.cloned.1.call-update) | async-done | bytes 524304 | tf_op jit(solution)/shard_map/reduce_scatter | solution.py:72
  493.2 1.9 add_convert_fusion
  (13 shorter events, 0.1 us)
Async XLA Ops:
  6.5 108.6 %copy-start = (f32[512,2]{0,1:T(2,128)S(1)}, f32[512,2]{0,1:T(2,128)}, u32[]{:S(2)}) copy-start(f32[512,2]{0,1:T(2,128)} %param.14) | copy-start | bytes 12292
  6.5 54.9 %all-gather.6.cloned.1.call-start = ((), (), s32[]{:S(2)}) async-start(), calls=%async_computation.2 | async-start | bytes 2359296 | tf_op jit(solution)/shard_map/all_gather | solution.py:23
  7.3 103.9 %all-gather.8.cloned.1.call-start = ((), (), s32[]{:S(2)}) async-start(), calls=%async_computation.3 | async-start | bytes 2359296 | tf_op jit(solution)/shard_map/all_gather | solution.py:24
  8.0 187.6 %all-gather.10.cloned.1.call-start = ((), (), s32[]{:S(2)}) async-start(), calls=%async_computation.4 | async-start | bytes 2621440 | tf_op jit(solution)/shard_map/all_gather | solution.py:63
  161.1 13.2 %copy-start.1 = (f32[2048]{0:T(1024)S(1)}, f32[2048]{0:T(1024)}, u32[]{:S(2)}) copy-start(f32[2048]{0:T(1024)} %param.17) | copy-start | bytes 24580
  175.3 146.8 %all-gather.12.cloned.1.call-start = ((), (), s32[]{:S(2)}) async-start(), calls=%async_computation.5 | async-start | bytes 9437184 | tf_op jit(solution)/shard_map/all_gather | solution.py:66
  175.8 271.3 %all-gather.14.cloned.1.call-start = ((), (), s32[]{:S(2)}) async-start(), calls=%async_computation.6 | async-start | bytes 9437184 | tf_op jit(solution)/shard_map/all_gather | solution.py:70
  176.4 316.7 %reduce-scatter.2.cloned.1.call-start = ((), (), s32[]{:S(2)}) async-start(), calls=%async_computation.7 | async-start | bytes 2621440 | tf_op jit(solution)/shard_map/reduce_scatter | solution.py:72
Sparse Core Ops, SparseCore 0:
  9.5 51.9 all-gather.5
  63.5 47.6 all-gather.7
  175.4 20.1 all-gather.9
  197.6 124.4 all-gather.11
  324.0 123.1 all-gather.13
  463.8 29.3 reduce-scatter.1
where the time goes:
time: 502 us
  waiting for transfers between devices  368 us (73%)
  matrix products  41.4 us (8%)
  blocking collectives  41.2 us (8%)
  local copies, waits for them, and re-layouts  18 us (4%)
  other arithmetic  16.3 us (3%)
  between operations  13.6 us (3%)
    all_gather x1, waiting for transfers between devices, per_device(): lax.all_gather(w_up, 'sp', axis=0, tiled=True)  126 us
    all_gather x1, waiting for transfers between devices, per_device(): down_whole = lax.all_gather(w_down, 'sp', axis=1, tiled=True)  125 us
    all_gather x1, waiting for transfers between devices, per_device(): value_rows = lax.all_gather(values, 'sp', axis=0, tiled=True)  45.8 us
    all_gather x1, blocking collectives, per_device(): all_gates = lax.all_gather(cum_gate, 'sp', axis=0, tiled=True)  32.7 us
    reduce_scatter x1, waiting for transfers between devices, per_device(): lax.psum_scatter(lax.optimization_barrier(rounded).astype(jnp.float32).as...  29.5 us
    all_gather x1, waiting for transfers between devices, per_device(): key_rows = lax.all_gather(keys, 'sp', axis=0, tiled=True)  19.4 us
    all_gather x1, waiting for transfers between devices, per_device(): normed_all = lax.all_gather(normed, 'tp', axis=0, tiled=True)  19 us
    dot_general x1, matrix products, per_device(): jnp.dot(hidden, down_whole, preferred_element_type=jnp.float32)  16.5 us
  transfers between devices with their start and end apart: 6, of which 6 were waited for; matrix products, arithmetic and copies ran while one was open for 1% of the time, Pallas kernels for 0%

commit v1 on v0

--- a/solution.py
+++ b/solution.py
@@ -13,7 +13,12 @@
     row_offset = lax.axis_index("sp") * tok_rows
     query_heads = queries.reshape(tok_rows, heads_here, head_size)
     query_pos = row_offset + jnp.arange(tok_rows, dtype=jnp.int32)
-    all_gates = lax.all_gather(cum_gate, "sp", axis=0, tiled=True)
+    ring = [cum_gate]
+    for hop in range(7):
+        ring.append(lax.ppermute(ring[-1], "sp", [(dev, (dev + 1) % 8) for dev in range(8)]))
+    all_gates = jnp.roll(
+        jnp.concatenate(ring[::-1], axis=0), (lax.axis_index("sp") + 1) * ring[0].shape[0], axis=0
+    )
     initial = (
         jnp.full((tok_rows, heads_here), -1e30, jnp.float32),
         jnp.zeros((tok_rows, heads_here), jnp.float32),

time: 502 us -> 503 us (level)
  blocking collectives: 41.2 us -> 8.55 us
  waiting for transfers between devices: 368 us -> 396 us
    ppermute x0 -> x7, waiting for transfers between devices: none -> 41.9 us  [per_device(): lax.ppermute(ring[-1], 'sp', [(dev, (dev + 1) % 8) for dev in range(8)])]
    all_gather x1 -> x0, blocking collectives: 32.7 us -> none  [per_device(): all_gates = lax.all_gather(cum_gate, 'sp', axis=0, tiled=True)]
    all_gather x1, waiting for transfers between devices: 19.4 us -> 5.61 us  [per_device(): key_rows = lax.all_gather(keys, 'sp', axis=0, tiled=True)]
  transfers between devices with their start and end apart: 6 -> 13, of which waited for: 6 -> 13; matrix products, arithmetic and copies ran while one was open for 1% -> 1% of each run, Pallas kernels for 0% -> 0%
where the time goes in v1:
time: 503 us; the launch traced here: 502 us
  waiting for transfers between devices  396 us (79%)
  matrix products  41.5 us (8%)
  local copies, waits for them, and re-layouts  19.5 us (4%)
  other arithmetic  16.3 us (3%)
  between operations  13.6 us (3%)
  blocking collectives  8.55 us (2%)
    all_gather x1, waiting for transfers between devices, per_device(): lax.all_gather(w_up, 'sp', axis=0, tiled=True)  126 us
    all_gather x1, waiting for transfers between devices, per_device(): down_whole = lax.all_gather(w_down, 'sp', axis=1, tiled=True)  125 us
    all_gather x1, waiting for transfers between devices, per_device(): value_rows = lax.all_gather(values, 'sp', axis=0, tiled=True)  45.7 us
    ppermute x7, waiting for transfers between devices, per_device(): lax.ppermute(ring[-1], 'sp', [(dev, (dev + 1) % 8) for dev in range(8)])  41.9 us
    reduce_scatter x1, waiting for transfers between devices, per_device(): lax.psum_scatter(lax.optimization_barrier(rounded).astype(jnp.float32).as...  29.5 us
    all_gather x1, waiting for transfers between devices, per_device(): normed_all = lax.all_gather(normed, 'tp', axis=0, tiled=True)  18.9 us
    dot_general x1, matrix products, per_device(): jnp.dot(hidden, down_whole, preferred_element_type=jnp.float32)  16.5 us
    dot_general x2, matrix products, absorb_block(): jnp.einsum('qhk,khd->qhd', weights.astype(jnp.bfloat16), value_blk, prefe...  12.6 us
  transfers between devices with their start and end apart: 13, of which 13 were waited for; matrix products, arithmetic and copies ran while one was open for 1% of the time, Pallas kernels for 0%

profile of v1, /device:TPU:0, one launch (start us, length us, event | category | flops | bytes accessed | tf_op | source)
XLA Modules:
  0.0 502.0 jit_solution(10361863315624895249)
XLA Ops:
  6.5 0.7 all-gather.6.cloned.1.call-update
  7.3 0.0 all-gather.8.cloned.1.call-start
  7.3 0.7 all-gather.8.cloned.1.call-update
  8.0 0.0 all-gather.10.cloned.1.call-start
  8.1 3.0 collective-permute-start
  11.1 4.8 collective-permute-done
  15.9 0.0 collective-permute-start.1
  15.9 6.3 %collective-permute-done.1 = f32[512,2]{0,1:T(2,128)S(1)} collective-permute-done((f32[512,2]{0,1:T(2,128)S(1)}, f32[512,2]{0,1:T(2,128)S(1)}, u32[]{:S(2)}, u32[]{:S(2)}) %collective-permute-start.1) | collective-permute-done | bytes 4128 | tf_op jit(solution)/shard_map/ppermute | solution.py:18
  22.2 0.0 collective-permute-start.2
  22.2 6.5 %collective-permute-done.2 = f32[512,2]{0,1:T(2,128)S(1)} collective-permute-done((f32[512,2]{0,1:T(2,128)S(1)}, f32[512,2]{0,1:T(2,128)S(1)}, u32[]{:S(2)}, u32[]{:S(2)}) %collective-permute-start.2) | collective-permute-done | bytes 4128 | tf_op jit(solution)/shard_map/ppermute | solution.py:18
  28.8 0.0 collective-permute-start.3
  28.8 6.3 %collective-permute-done.3 = f32[512,2]{0,1:T(2,128)S(1)} collective-permute-done((f32[512,2]{0,1:T(2,128)S(1)}, f32[512,2]{0,1:T(2,128)S(1)}, u32[]{:S(2)}, u32[]{:S(2)}) %collective-permute-start.3) | collective-permute-done | bytes 4128 | tf_op jit(solution)/shard_map/ppermute | solution.py:18
  35.1 0.0 collective-permute-start.4
  35.1 6.4 %collective-permute-done.4 = f32[512,2]{0,1:T(2,128)S(1)} collective-permute-done((f32[512,2]{0,1:T(2,128)S(1)}, f32[512,2]{0,1:T(2,128)S(1)}, u32[]{:S(2)}, u32[]{:S(2)}) %collective-permute-start.4) | collective-permute-done | bytes 4128 | tf_op jit(solution)/shard_map/ppermute | solution.py:18
  41.5 0.0 collective-permute-start.5
  41.5 6.5 %collective-permute-done.5 = f32[512,2]{0,1:T(2,128)S(1)} collective-permute-done((f32[512,2]{0,1:T(2,128)S(1)}, f32[512,2]{0,1:T(2,128)S(1)}, u32[]{:S(2)}, u32[]{:S(2)}) %collective-permute-start.5) | collective-permute-done | bytes 4128 | tf_op jit(solution)/shard_map/ppermute | solution.py:18
  48.0 1.1 copy.17
  49.1 0.2 copy.19
  49.3 5.0 collective-permute-done.6
  54.4 0.7 constant_dynamic-update-slice_fusion.8
  55.1 0.7 constant_dynamic-update-slice_fusion
  55.8 5.6 %all-gather.6.cloned.1.call-done = bf16[4096,256]{1,0:T(8,128)(2,1)} async-done(((bf16[512,256]{1,0:T(8,128)(2,1)}), bf16[4096,256]{1,0:T(8,128)(2,1)}) %all-gather.6.cloned.1.call-update) | async-done | bytes 2097168 | tf_op jit(solution)/shard_map/all_gather | solution.py:28
  61.5 4.0 reshape.62
  65.5 45.7 %all-gather.8.cloned.1.call-done = bf16[4096,256]{1,0:T(8,128)(2,1)} async-done(((bf16[512,256]{1,0:T(8,128)(2,1)}), bf16[4096,256]{1,0:T(8,128)(2,1)}) %all-gather.8.cloned.1.call-update) | async-done | bytes 2097168 | tf_op jit(solution)/shard_map/all_gather | solution.py:29
  111.3 4.0 reshape.64
  115.2 45.9 %while.15 = (s32[]{:T(128)}, f32[512,2]{0,1:T(2,128)S(1)}, f32[512,2]{0,1:T(2,128)S(1)}, f32[512,2,128]{0,2,1:T(8,128)}, s32[2]{0:T(128)S(1)}, /*index=5*/bf16[2...) while((s32[]{:T(128)}, f32[512,2]{0,1:T(2,128)S(1)}, ...), condition=%wide.region_3.4_spmd.clone, body=%wide.region_0.3_spmd.clone.sunk | while | flops 1110842880 | bytes 39239884 | solution.py:60
  115.2 0.6 dynamic_slice.32
  117.5 0.1 dynamic-slice_bitcast_fusion.2
  117.6 0.6 iota_add_fusion.5
  118.2 0.8 broadcast_compare_fusion.2
  118.9 2.7 constant_dynamic-slice_fusion.4
  121.6 4.6 fusion.40
  126.3 4.8 fusion.42
  131.1 0.8 copy.34
  131.9 6.2 %fusion.44 = f32[512,2,128]{0,2,1:T(8,128)} fusion(f32[2,2048,512]{2,1,0:T(8,128)} %get-tuple-element.231, f32[512,2]{0,1:T(2,128)S(1)} %fusion.41, f32[2,2048]{1,0:T(2,128)S(1)} %dynamic-slice_bitcast_fusion.2, f32[512,2]{0,1:T(2,128)S(1)} %get-tuple-element.270, pred[512,2048]{0,1:T(8,128)(4,1)S(1)} %broadcast_compare_fusion.2, ...), kind=kOutput, calls=%fused_computation.12.clone.1 | convolution fusion | flops 549847040 | bytes 11563009 | tf_op jit(solution)/shard_map/while/body/eval_jaxpr/qhk,khd->qhd/dot_general | solution.py:51
  138.1 0.6 dynamic_slice.32
  140.4 0.1 dynamic-slice_bitcast_fusion.2
  140.5 0.6 iota_add_fusion.5
  141.1 0.8 broadcast_compare_fusion.2
  141.8 2.7 constant_dynamic-slice_fusion.4
  144.5 4.6 fusion.40
  149.2 4.8 fusion.42
  154.0 0.8 copy.34
  154.8 6.4 %fusion.44 = f32[512,2,128]{0,2,1:T(8,128)} fusion(f32[2,2048,512]{2,1,0:T(8,128)} %get-tuple-element.231, f32[512,2]{0,1:T(2,128)S(1)} %fusion.41, f32[2,2048]{1,0:T(2,128)S(1)} %dynamic-slice_bitcast_fusion.2, f32[512,2]{0,1:T(2,128)S(1)} %get-tuple-element.270, pred[512,2048]{0,1:T(8,128)(4,1)S(1)} %broadcast_compare_fusion.2, ...), kind=kOutput, calls=%fused_computation.12.clone.1 | convolution fusion | flops 549847040 | bytes 11563009 | tf_op jit(solution)/shard_map/while/body/eval_jaxpr/qhk,khd->qhd/dot_general | solution.py:51
  161.1 1.1 divide_convert_fusion
  162.2 0.1 reshape.65
  162.3 0.2 copy.24
  162.5 8.5 %all_to_all.16 = bf16[4,128,256]{2,1,0:T(8,128)(2,1)S(1)} all-to-all(bf16[4,128,256]{2,1,0:T(8,128)(2,1)S(1)} %copy.24), channel_id=1, replica_groups=mesh['sp'=8,'tp'=4] {'tp'}, dimensions={0} | all-to-all | bytes 524288 | tf_op jit(solution)/shard_map/all_to_all | solution.py:63
  171.0 0.2 copy.22
  171.2 3.1 multiply_reduce_fusion
  174.4 0.9 multiply_convert_fusion.1
  175.3 0.0 all-gather.10.cloned.1.call-update
  175.3 0.0 all-gather.12.cloned.1.call-start
  175.4 0.5 all-gather.12.cloned.1.call-update
  175.9 0.0 all-gather.14.cloned.1.call-start
  176.0 0.5 all-gather.14.cloned.1.call-update
  176.5 0.2 reduce-scatter.2.cloned.1.call-start
  176.7 18.9 %all-gather.10.cloned.1.call-done = bf16[512,2048]{1,0:T(8,128)(2,1)} async-done(((bf16[128,2048]{1,0:T(8,128)(2,1)}), bf16[512,2048]{1,0:T(8,128)(2,1)}) %all-gather.10.cloned.1.call-update) | async-done | bytes 2097168 | tf_op jit(solution)/shard_map/all_gather | solution.py:68
  195.7 126.5 %all-gather.12.cloned.1.call-done = bf16[2048,2048]{1,0:T(8,128)(2,1)} async-done(((bf16[256,2048]{1,0:T(8,128)(2,1)}), bf16[2048,2048]{1,0:T(8,128)(2,1)}) %all-gather.12.cloned.1.call-update) | async-done | bytes 8388624 | tf_op jit(solution)/shard_map/all_gather | solution.py:71
  322.2 125.0 %all-gather.14.cloned.1.call-done = bf16[2048,2048]{1,0:T(8,128)(2,1)} async-done(((bf16[2048,256]{1,0:T(8,128)(2,1)}), bf16[2048,2048]{1,0:T(8,128)(2,1)}) %all-gather.14.cloned.1.call-update) | async-done | bytes 8388624 | tf_op jit(solution)/shard_map/all_gather | solution.py:75
  447.2 16.5 %convolution_convert_fusion = bf16[512,2048]{1,0:T(8,128)(2,1)} fusion(bf16[2048,2048]{1,0:T(8,128)(2,1)} %all-gather.14.cloned.1.call-done, bf16[512,2048]{1,0:T(8,128)(2,1)} %all-gather.10.cloned.1.call-done, bf16[2048,2048]{1,0:T(8,128)(2,1)} %all-gather.12.cloned.1.call-done), kind=kOutput, calls=%fused_computation.30 | convolution fusion | flops 8594128896 | bytes 20971520 | tf_op jit(solution)/shard_map/dot_general | solution.py:76
  463.7 0.0 reduce-scatter.2.cloned.1.call-update
  463.7 29.5 %reduce-scatter.2.cloned.1.call-done = bf16[128,2048]{1,0:T(8,128)(2,1)} async-done(((bf16[512,2048]{1,0:T(8,128)(2,1)}), bf16[128,2048]{1,0:T(8,128)(2,1)}) %reduce-scatter.2.cloned.1.call-update) | async-done | bytes 524304 | tf_op jit(solution)/shard_map/reduce_scatter | solution.py:77
  493.2 1.9 add_convert_fusion
  (34 shorter events, 0.2 us)
Async XLA Ops:
  6.5 108.7 %copy-start = (f32[512,2]{0,1:T(2,128)S(1)}, f32[512,2]{0,1:T(2,128)}, u32[]{:S(2)}) copy-start(f32[512,2]{0,1:T(2,128)} %param.14) | copy-start | bytes 12292
  6.5 54.9 %all-gather.6.cloned.1.call-start = ((), (), s32[]{:S(2)}) async-start(), calls=%async_computation.2 | async-start | bytes 2359296 | tf_op jit(solution)/shard_map/all_gather | solution.py:28
  7.3 104.0 %all-gather.8.cloned.1.call-start = ((), (), s32[]{:S(2)}) async-start(), calls=%async_computation.3 | async-start | bytes 2359296 | tf_op jit(solution)/shard_map/all_gather | solution.py:29
  8.0 187.7 %all-gather.10.cloned.1.call-start = ((), (), s32[]{:S(2)}) async-start(), calls=%async_computation.4 | async-start | bytes 2621440 | tf_op jit(solution)/shard_map/all_gather | solution.py:68
  8.1 7.9 %collective-permute-start = (f32[512,2]{0,1:T(2,128)}, f32[512,2]{0,1:T(2,128)S(1)}, u32[]{:S(2)}, u32[]{:S(2)}) collective-permute-start(f32[512,2]{0,1:T(2,128)} %param.14), channel_id=1, source_target_pairs={{0,4},{4,8},{8,12},{12,16},{16,20},{20,24},{24,28},{28,0},{1,5},{5... | collective-permute-start | bytes 12296 | tf_op jit(solution)/shard_map/ppermute | solution.py:18
  15.9 6.3 %collective-permute-start.1 = (f32[512,2]{0,1:T(2,128)S(1)}, f32[512,2]{0,1:T(2,128)S(1)}, u32[]{:S(2)}, u32[]{:S(2)}) collective-permute-start(f32[512,2]{0,1:T(2,128)S(1)} %collective-permute-done), channel_id=1, source_target_pairs={{0,4},{4,8},{8,12},{12,16},{16,20},{20,24},{24,28},{28,0},{1,5},{5... | collective-permute-start | bytes 12296 | tf_op jit(solution)/shard_map/ppermute | solution.py:18
  22.2 6.5 %collective-permute-start.2 = (f32[512,2]{0,1:T(2,128)S(1)}, f32[512,2]{0,1:T(2,128)S(1)}, u32[]{:S(2)}, u32[]{:S(2)}) collective-permute-start(f32[512,2]{0,1:T(2,128)S(1)} %collective-permute-done.1), channel_id=1, source_target_pairs={{0,4},{4,8},{8,12},{12,16},{16,20},{20,24},{24,28},{28,0},{1,5},{5... | collective-permute-start | bytes 12296 | tf_op jit(solution)/shard_map/ppermute | solution.py:18
  28.8 6.3 %collective-permute-start.3 = (f32[512,2]{0,1:T(2,128)S(1)}, f32[512,2]{0,1:T(2,128)S(1)}, u32[]{:S(2)}, u32[]{:S(2)}) collective-permute-start(f32[512,2]{0,1:T(2,128)S(1)} %collective-permute-done.2), channel_id=1, source_target_pairs={{0,4},{4,8},{8,12},{12,16},{16,20},{20,24},{24,28},{28,0},{1,5},{5... | collective-permute-start | bytes 12296 | tf_op jit(solution)/shard_map/ppermute | solution.py:18
  35.1 6.4 %collective-permute-start.4 = (f32[512,2]{0,1:T(2,128)S(1)}, f32[512,2]{0,1:T(2,128)S(1)}, u32[]{:S(2)}, u32[]{:S(2)}) collective-permute-start(f32[512,2]{0,1:T(2,128)S(1)} %collective-permute-done.3), channel_id=1, source_target_pairs={{0,4},{4,8},{8,12},{12,16},{16,20},{20,24},{24,28},{28,0},{1,5},{5... | collective-permute-start | bytes 12296 | tf_op jit(solution)/shard_map/ppermute | solution.py:18
  41.5 6.5 %collective-permute-start.5 = (f32[512,2]{0,1:T(2,128)S(1)}, f32[512,2]{0,1:T(2,128)S(1)}, u32[]{:S(2)}, u32[]{:S(2)}) collective-permute-start(f32[512,2]{0,1:T(2,128)S(1)} %collective-permute-done.4), channel_id=1, source_target_pairs={{0,4},{4,8},{8,12},{12,16},{16,20},{20,24},{24,28},{28,0},{1,5},{5... | collective-permute-start | bytes 12296 | tf_op jit(solution)/shard_map/ppermute | solution.py:18
  48.0 6.3 %collective-permute-start.6 = (f32[512,2]{0,1:T(2,128)S(1)}, f32[512,2]{0,1:T(2,128)S(1)}, u32[]{:S(2)}, u32[]{:S(2)}) collective-permute-start(f32[512,2]{0,1:T(2,128)S(1)} %collective-permute-done.5), channel_id=1, source_target_pairs={{0,4},{4,8},{8,12},{12,16},{16,20},{20,24},{24,28},{28,0},{1,5},{5... | collective-permute-start | bytes 12296 | tf_op jit(solution)/shard_map/ppermute | solution.py:18
  161.1 13.2 %copy-start.1 = (f32[2048]{0:T(1024)S(1)}, f32[2048]{0:T(1024)}, u32[]{:S(2)}) copy-start(f32[2048]{0:T(1024)} %param.17) | copy-start | bytes 24580
  175.3 146.8 %all-gather.12.cloned.1.call-start = ((), (), s32[]{:S(2)}) async-start(), calls=%async_computation.5 | async-start | bytes 9437184 | tf_op jit(solution)/shard_map/all_gather | solution.py:71
  175.9 271.3 %all-gather.14.cloned.1.call-start = ((), (), s32[]{:S(2)}) async-start(), calls=%async_computation.6 | async-start | bytes 9437184 | tf_op jit(solution)/shard_map/all_gather | solution.py:75
  176.5 316.7 %reduce-scatter.2.cloned.1.call-start = ((), (), s32[]{:S(2)}) async-start(), calls=%async_computation.7 | async-start | bytes 2621440 | tf_op jit(solution)/shard_map/reduce_scatter | solution.py:77
Sparse Core Ops, SparseCore 0:
  9.5 51.9 all-gather.5
  63.6 47.6 all-gather.7
  175.5 20.1 all-gather.9
  197.7 124.4 all-gather.11
  324.1 123.1 all-gather.13
  463.9 29.3 reduce-scatter.1
